TPU v7x, 256 devices: a whole 4x4x8 slice. The times are simulated.
256 devices in a mesh: ep: 64 (over z, x, core), tp: 4 (over y).
Axes of the slice: x: 4, y: 4, z: 8, core: 2. Of those that a mesh axis runs over, the one named last changes fastest.
Arguments:
- query_rows: bfloat16 [16384, 1024], P('ep', 'tp'), may hold values from -8 to 8
- key_rows: bfloat16 [16384, 256], P('ep', 'tp'), may hold values from -8 to 8
- value_rows: bfloat16 [16384, 256], P('ep', 'tp'), may hold values from -16 to 16
- query_gain: float32 [64], replicated, may hold values from 0.5 to 7.5
- key_gain: float32 [64], replicated, may hold values from 0.5 to 7.5
- moe_tokens: bfloat16 [32768, 2048], P(('ep', 'tp')), may hold values from -6 to 6
- norm_gain: float32 [2048], replicated, may hold values from 0.1 to 1.9
- routes: int32 [32768, 2], P('ep'), may hold values from 0 to 63, all different within a row; in each aligned block of 128 rows (0 to 127, 128 to 255, ...) at most 8 rows name the same one
- route_weights: float32 [32768, 2], P('ep'), may hold values from 0.1 to 1
- expert_gate: bfloat16 [64, 2048, 1024], P('ep', None, 'tp'), may hold values from -0.125 to 0.125
- expert_up: bfloat16 [64, 2048, 1024], P('ep', None, 'tp'), may hold values from -0.125 to 0.125
- expert_down: bfloat16 [64, 1024, 2048], P('ep', 'tp'), may hold values from -0.1875 to 0.1875
- shared_gate: bfloat16 [2048, 1024], P(None, 'tp'), may hold values from -0.125 to 0.125
- shared_up: bfloat16 [2048, 1024], P(None, 'tp'), may hold values from -0.125 to 0.125
- shared_down: bfloat16 [1024, 2048], P('tp'), may hold values from -0.1875 to 0.1875
Outputs:
- attn_out: bfloat16 [16384, 1024], P('ep', 'tp')
- moe_out: bfloat16 [32768, 2048], P(('ep', 'tp'))
Inputs may be any that keep to these rules, and one draw needn't show every extreme that they name: `routes`: each row names 2 different experts. Within each aligned block of 128 rows no expert is named more than 8 times, and in every draw some expert is named exactly 8 times in some block.
All inputs are finite; a program needn't handle non-finite values.
Results may differ from a plain program's by a relative error of at most 0.012.
The roundings to bfloat16 on the way count: a program that leaves them out, or rounds other values in their place, can miss the bound.
Values may be sent and summed in bfloat16 or wider, within the bound.
A program may use at most 192 MiB of HBM per device.

v0:
```python
import functools

import jax
import jax.numpy as jnp
from jax import lax
from jax.experimental import pallas as pl
from jax.experimental.pallas import tpu as pltpu
from jax.sharding import PartitionSpec as P

GRID_W = 64
MESH = pl.DeviceIdType.MESH
F32 = jnp.float32
BF16 = jnp.bfloat16

epsilon = 1e-06
rotary_base = 10000.0
routed_scale = 2.5

N_Z, N_X, N_CORE = 8, 4, 2
N_EP, N_TP = 64, 4
CAP = 8
CHUNKS = 4
NT = (((1,), (1,)), ((), ()))


def prep_kernel(q_ref, kv_ref, qg_ref, kg_ref, cos_ref, sin_ref, qo_ref, kvo_ref):
    rows = q_ref.shape[0]
    lane = lax.broadcasted_iota(jnp.int32, (rows, 128), 1)
    low = lane < 64
    even = lax.rem(lane, 2) == 0
    cosine, sine = cos_ref[...], sin_ref[...]

    def turned(x, gain):
        squares = x * x
        first = jnp.sum(jnp.where(low, squares, 0.0), axis=1, keepdims=True) / 64.0
        second = jnp.sum(jnp.where(low, 0.0, squares), axis=1, keepdims=True) / 64.0
        inverse = jnp.where(low, lax.rsqrt(first + epsilon), lax.rsqrt(second + epsilon))
        y = x * inverse * gain
        partner = jnp.where(even, -pltpu.roll(y, 127, 1), pltpu.roll(y, 1, 1))
        return (y * cosine + partner * sine).astype(BF16).astype(F32)

    gain = qg_ref[...]
    for pair in range(q_ref.shape[1] // 128):
        x = q_ref[:, pair * 128 : pair * 128 + 128].astype(F32)
        out = turned(x, gain) * 0.125
        base = 2 * pair * rows
        qo_ref[base : base + rows, :] = jnp.where(low, out, 0.0).astype(BF16)
        qo_ref[base + rows : base + 2 * rows, :] = jnp.where(
            low, pltpu.roll(out, 64, 1), 0.0
        ).astype(BF16)
    kv = kv_ref[...].astype(F32)
    kvo_ref[...] = jnp.where(low, turned(kv, kg_ref[...]), kv).astype(BF16)


def prepared(query_rows, key_rows, value_rows, query_gain, key_gain):
    rows = query_rows.shape[0]
    positions = lax.axis_index("ep") * rows + jnp.arange(rows, dtype=jnp.int32)
    pair_count = 16
    inv_freq = rotary_base ** (-jnp.arange(pair_count, dtype=F32) / pair_count)
    grid_row = (positions // GRID_W).astype(F32)
    grid_col = (positions % GRID_W).astype(F32)
    angles = jnp.concatenate([grid_row[:, None] * inv_freq, grid_col[:, None] * inv_freq], axis=-1)
    angles = jnp.tile(jnp.repeat(angles, 2, axis=1), (1, 2))
    kv = jnp.concatenate([key_rows, value_rows], axis=1)
    return pl.pallas_call(
        prep_kernel,
        out_shape=[
            jax.ShapeDtypeStruct((4 * rows, 128), BF16),
            jax.ShapeDtypeStruct((rows, 128), BF16),
        ],
        name="prep",
    )(
        query_rows,
        kv,
        jnp.tile(query_gain[None, :], (1, 2)),
        jnp.tile(key_gain[None, :], (1, 2)),
        jnp.cos(angles),
        jnp.sin(angles),
    )


def silu_times(gate, up):
    return (gate / (1.0 + jnp.exp(-gate)) * up).astype(BF16)


def layer_kernel(
    q_ref, kv_ref, send_ref, normed_ref, choose_ref, gates_ref,
    wg_ref, wu_ref, wd_ref, sg_ref, su_ref, sd_ref,
    attn_ref, moe_ref,
    kvb, run_max, run_sum, mixed,
    wgb, wub, wdb, nall, arrived, rows_bf, hidden, outbuf, ret,
    sgb, sub, sdb, part, parts,
    item_send, item_recv, kv_send, kv_recv, x_send, x_recv, core_send, core_recv,
    disp_send, disp_recv, ret_send, ret_recv, rs_send, rs_recv, own_sem,
):
    me, lane = lax.axis_index("ep"), lax.axis_index("tp")
    z, x, c = lax.div(me, 8), lax.rem(lax.div(me, 2), 4), lax.rem(me, 2)
    right, left = lax.rem(lane + 1, N_TP), lax.rem(lane + 3, N_TP)
    opposite = lax.rem(lane + 2, N_TP)

    def at(zz, xx, cc):
        return (zz * N_X + xx) * N_CORE + cc

    def remote(src, dst, send_sem, recv_sem, axis, peer):
        return pltpu.make_async_remote_copy(
            src_ref=src, dst_ref=dst, send_sem=send_sem, recv_sem=recv_sem,
            device_id={axis: peer}, device_id_type=MESH,
        )

    barrier = pltpu.get_barrier_semaphore()

    def greet(i, carry):
        pl.semaphore_signal(
            barrier, inc=1, device_id={"ep": lax.rem(me + i, N_EP)}, device_id_type=MESH
        )
        return carry

    for i in range(1, N_TP):
        pl.semaphore_signal(
            barrier, inc=1, device_id={"tp": lax.rem(lane + i, N_TP)}, device_id_type=MESH
        )
    lax.fori_loop(1, N_EP, greet, 0)
    pl.semaphore_wait(barrier, N_EP - 1 + N_TP - 1)

    items = []
    for ref, buf in ((wg_ref, wgb), (wu_ref, wub)):
        for h in range(2):
            items.append((ref.at[pl.ds(h * 1024, 1024)], buf, (pl.ds(h * 1024, 1024),), h * 1024, 512))
    for j in range(CHUNKS):
        items.append((wd_ref.at[:, pl.ds(j * 512, 512)], wdb, (j,), 0, 128))
    items.append((normed_ref, nall, (), 0, 64))

    def item_copy(i, n):
        src, buf, where, base, half = items[i]
        lead = where[:-1] if where and not isinstance(where[0], int) else where
        s, r = item_send.at[i], item_recv.at[i]
        lower, upper = pl.ds(base, half), pl.ds(base + half, half)

        def piece(slot, rows):
            return buf.at[(slot,) + lead + (rows,)]

        if n == 0:
            return remote(src, buf.at[(1,) + where], s.at[0], r.at[0], "tp", right)
        if n == 1:
            return remote(src, buf.at[(2,) + where], s.at[1], r.at[1], "tp", left)
        if n == 2:
            return remote(piece(1, lower), piece(3, lower), s.at[2], r.at[2], "tp", right)
        return remote(piece(2, upper), piece(3, upper), s.at[3], r.at[3], "tp", left)

    def begin(i):
        if i < len(items):
            item_copy(i, 0).start()
            item_copy(i, 1).start()

    def service(i):
        item_copy(i, 0).wait_recv()
        item_copy(i, 2).start()
        item_copy(i, 1).wait_recv()
        item_copy(i, 3).start()
        begin(i + 2)

    def complete(i):
        item_copy(i, 2).wait_recv()
        item_copy(i, 3).wait_recv()

    begin(0)
    begin(1)

    local = [pltpu.make_async_copy(kv_ref, kvb.at[c, x, z], own_sem.at[0])]
    for n, (src, dst) in enumerate((
        (wg_ref, wgb.at[0]), (wu_ref, wub.at[0]), (sg_ref, sgb), (su_ref, sub), (sd_ref, sdb),
        (normed_ref, nall.at[0]), (send_ref.at[me], arrived.at[me]),
    )):
        local.append(pltpu.make_async_copy(src, dst, own_sem.at[n + 1]))
    for j in range(CHUNKS):
        local.append(pltpu.make_async_copy(
            wd_ref.at[:, pl.ds(j * 512, 512)], wdb.at[0, j], own_sem.at[8 + j]
        ))

    def along_z(i):
        return remote(
            kv_ref, kvb.at[c, x, z], kv_send.at[i], kv_recv.at[i],
            "ep", at(lax.rem(z + i, N_Z), x, c),
        )

    local[0].start()
    for i in range(1, N_Z):
        along_z(i).start()
    for copy in local[1:]:
        copy.start()

    x_next, x_prev = lax.rem(x + 1, N_X), lax.rem(x + 3, N_X)
    x_far = lax.rem(x + 2, N_X)
    up_x, down_x = at(z, x_next, c), at(z, x_prev, c)
    low_z, high_z = pl.ds(0, 4), pl.ds(4, 4)
    to_next = remote(kvb.at[c, x], kvb.at[c, x], x_send.at[0], x_recv.at[0], "ep", up_x)
    to_prev = remote(kvb.at[c, x], kvb.at[c, x], x_send.at[1], x_recv.at[1], "ep", down_x)
    on_next = remote(
        kvb.at[c, x_prev, low_z], kvb.at[c, x_prev, low_z], x_send.at[2], x_recv.at[2], "ep", up_x
    )
    on_prev = remote(
        kvb.at[c, x_next, high_z], kvb.at[c, x_next, high_z], x_send.at[3], x_recv.at[3], "ep", down_x
    )

    def to_core(block, n):
        return remote(
            kvb.at[c, block], kvb.at[c, block], core_send.at[n], core_recv.at[n],
            "ep", at(z, x, 1 - c),
        )

    blocks = (x, x_next, x_prev, x_far)

    local[0].wait()
    for i in range(1, N_Z):
        along_z(i).wait_recv()
    to_next.start()
    to_prev.start()
    to_core(blocks[0], 0).start()

    def dispatch(i, carry):
        peer = lax.rem(me + i, N_EP)
        remote(
            send_ref.at[peer], arrived.at[me], disp_send.at[0], disp_recv.at[0], "ep", peer
        ).start()
        return carry

    lax.fori_loop(1, N_EP, dispatch, 0)

    service(0)

    run_max[...] = jnp.full_like(run_max, -jnp.inf)
    run_sum[...] = jnp.zeros_like(run_sum)
    mixed[...] = jnp.zeros_like(mixed)

    def attention_step(t, carry):
        xi = lax.div(t, 2)
        x_rel = xi + lax.div(xi, 2) - 2 * lax.div(xi, 3)
        block = lax.rem(x + x_rel, N_X)
        core = lax.rem(c + lax.rem(t, 2), N_CORE)

        @pl.when(t == 1)
        def _():
            to_core(blocks[0], 0).wait_recv()

        @pl.when(t == 2)
        def _():
            to_prev.wait_recv()
            on_prev.start()
            to_core(x_next, 1).start()
            to_next.wait_recv()
            on_next.start()
            to_core(x_prev, 2).start()

        @pl.when(t == 3)
        def _():
            service(1)
            to_core(x_next, 1).wait_recv()

        @pl.when(t == 5)
        def _():
            to_core(x_prev, 2).wait_recv()

        @pl.when(t == 6)
        def _():
            on_next.wait_recv()
            on_prev.wait_recv()
            to_core(x_far, 3).start()

        @pl.when(t == 7)
        def _():
            service(2)
            to_core(x_far, 3).wait_recv()

        keys = kvb[core, block].reshape(N_Z * 256, 128)
        for qb in range(4):
            rows = slice(qb * 256, qb * 256 + 256)
            scores = lax.dot_general(q_ref[rows], keys, NT, preferred_element_type=F32)
            old = run_max[rows]
            new = jnp.maximum(old, jnp.max(scores, axis=1, keepdims=True))
            factor = jnp.exp(old - new)
            weights = jnp.exp(scores - new[:, :1])
            total = run_sum[rows] * factor
            for n in range(N_Z * 256 // 128):
                total = total + weights[:, n * 128 : n * 128 + 128]
            run_sum[rows] = total
            run_max[rows] = new
            mixed[rows] = mixed[rows] * factor + jnp.dot(
                weights.astype(BF16), keys, preferred_element_type=F32
            )
        return carry

    lax.fori_loop(0, 8, attention_step, 0)

    low = lax.broadcasted_iota(jnp.int32, (256, 128), 1) < 64
    for pair in range(2):
        base = pair * 512
        halves = []
        for h in range(2):
            rows = slice(base + h * 256, base + h * 256 + 256)
            halves.append(mixed[rows] / jnp.sum(run_sum[rows], axis=1, keepdims=True))
        attn_ref[:, pair * 128 : pair * 128 + 128] = jnp.where(
            low, pltpu.roll(halves[0], 64, 1), halves[1]
        ).astype(BF16)

    service(3)
    for copy in local[1:]:
        copy.wait()
    remote(
        send_ref.at[pl.ds(0, N_EP - 1)], arrived.at[pl.ds(0, N_EP - 1)],
        disp_send.at[0], disp_recv.at[0], "ep", up_x,
    ).wait()
    rows_bf[...] = arrived[...].astype(F32).reshape(N_EP * CAP, -1).astype(BF16)

    for slot in range(N_TP):
        if slot == 2:
            service(4)
        if slot == 3:
            for i in range(4):
                complete(i)
        rows_in = rows_bf[...]
        gate = jnp.dot(rows_in, wgb[slot], preferred_element_type=F32)
        up = jnp.dot(rows_in, wub[slot], preferred_element_type=F32)
        hidden[slot] = silu_times(gate, up)

    def send_back(j):
        def one(i, carry):
            peer = lax.rem(me + i, N_EP)
            remote(
                outbuf.at[j, peer], ret.at[j, me], ret_send.at[j], ret_recv.at[j], "ep", peer
            ).start()
            return carry

        lax.fori_loop(1, N_EP, one, 0)

    back = []
    for j in range(CHUNKS):
        service(5 + j)
        complete(4 + j)
        total = jnp.zeros((N_EP * CAP, 512), F32)
        for slot in range(N_TP):
            total = total + jnp.dot(
                hidden[slot], wdb[slot, j], preferred_element_type=F32
            ).astype(BF16).astype(F32)
        outbuf[j] = total.reshape(N_EP, CAP, 512).astype(BF16)
        send_back(j)
        copy = pltpu.make_async_copy(outbuf.at[j, me], ret.at[j, me], own_sem.at[12 + j])
        copy.start()
        back.append(copy)

    def shared_of(slot):
        rows_in = nall[slot]
        gate = jnp.dot(rows_in, sgb[...], preferred_element_type=F32)
        up = jnp.dot(rows_in, sub[...], preferred_element_type=F32)
        return jnp.dot(silu_times(gate, up), sdb[...], preferred_element_type=F32).astype(BF16)

    shares = {
        1: remote(part.at[1], parts.at[2], rs_send.at[1], rs_recv.at[2], "tp", left),
        2: remote(part.at[2], parts.at[1], rs_send.at[2], rs_recv.at[1], "tp", right),
        3: remote(part.at[3], parts.at[3], rs_send.at[3], rs_recv.at[3], "tp", opposite),
    }
    for slot in (1, 2):
        part[slot] = shared_of(slot)
        shares[slot].start()
    complete(8)
    part[3] = shared_of(3)
    shares[3].start()
    part[0] = shared_of(0)
    for slot in (1, 2, 3):
        shares[slot].wait_recv()

    for j in range(CHUNKS):
        columns = slice(j * 512, j * 512 + 512)
        back[j].wait()
        remote(
            outbuf.at[j, pl.ds(0, N_EP - 1)], ret.at[j, pl.ds(0, N_EP - 1)],
            ret_send.at[j], ret_recv.at[j], "ep", up_x,
        ).wait()
        flat = ret[j].astype(F32).reshape(N_EP * CAP, 512).astype(BF16)
        total = part[0, :, columns].astype(F32)
        for slot in (1, 2, 3):
            total = total + parts[slot, :, columns].astype(F32)
        for k in range(2):
            picked = jnp.dot(choose_ref[k], flat, preferred_element_type=F32)
            total = total + gates_ref[:, k : k + 1] * picked
        moe_ref[:, columns] = total.astype(BF16)

    for i in range(len(items)):
        for n in range(4):
            item_copy(i, n).wait_send()
    for i in range(1, N_Z):
        along_z(i).wait_send()
    for copy in (to_next, to_prev, on_next, on_prev):
        copy.wait_send()
    for n in range(4):
        to_core(blocks[n], n).wait_send()
    for slot in (1, 2, 3):
        shares[slot].wait_send()


def layer(q, kv, send, normed, choose, gates, wg, wu, wd, sg, su, sd):
    vmem = pl.BlockSpec(memory_space=pltpu.VMEM)
    anywhere = pl.BlockSpec(memory_space=pl.ANY)
    width = normed.shape[1]
    dma = pltpu.SemaphoreType.DMA
    return pl.pallas_call(
        layer_kernel,
        out_shape=[
            jax.ShapeDtypeStruct((256, 256), BF16),
            jax.ShapeDtypeStruct(normed.shape, BF16),
        ],
        in_specs=[vmem, anywhere, anywhere, anywhere, vmem, vmem] + [anywhere] * 6,
        out_specs=[vmem, vmem],
        scratch_shapes=[
            pltpu.VMEM((N_CORE, N_X, N_Z, 256, 128), BF16),
            pltpu.VMEM((1024, 128), F32),
            pltpu.VMEM((1024, 128), F32),
            pltpu.VMEM((1024, 128), F32),
            pltpu.VMEM((N_TP, width, 256), BF16),
            pltpu.VMEM((N_TP, width, 256), BF16),
            pltpu.VMEM((N_TP, CHUNKS, 256, 512), BF16),
            pltpu.VMEM((N_TP, 128, width), BF16),
            pltpu.VMEM((N_EP, CAP, width), BF16),
            pltpu.VMEM((N_EP * CAP, width), BF16),
            pltpu.VMEM((N_TP, N_EP * CAP, 256), BF16),
            pltpu.VMEM((CHUNKS, N_EP, CAP, 512), BF16),
            pltpu.VMEM((CHUNKS, N_EP, CAP, 512), BF16),
            pltpu.VMEM((width, 256), BF16),
            pltpu.VMEM((width, 256), BF16),
            pltpu.VMEM((256, width), BF16),
            pltpu.VMEM((N_TP, 128, width), BF16),
            pltpu.VMEM((N_TP, 128, width), BF16),
            dma((9, 4)), dma((9, 4)), dma((N_Z,)), dma((N_Z,)), dma((4,)), dma((4,)),
            dma((4,)), dma((4,)), dma((1,)), dma((1,)), dma((CHUNKS,)), dma((CHUNKS,)),
            dma((4,)), dma((4,)), dma((16,)),
        ],
        compiler_params=pltpu.CompilerParams(
            collective_id=1, has_side_effects=True, vmem_limit_bytes=60 * 1024 * 1024
        ),
        name="layer",
    )(q, kv, send, normed, choose, gates, wg, wu, wd, sg, su, sd)


def slot_numbers(own_routes, experts, capacity):
    tok_rows = own_routes.shape[0]
    named = own_routes[:, :, None] == jnp.arange(experts, dtype=jnp.int32)
    counts = jnp.any(named, axis=1).astype(BF16)
    rows = jnp.arange(tok_rows, dtype=jnp.int32)
    before = (rows[:, None] > rows[None, :]).astype(BF16)
    earlier = jnp.dot(before, counts, preferred_element_type=F32)
    ranks = jnp.sum(jnp.where(named, earlier[:, None, :], 0.0), axis=2).astype(jnp.int32)
    return own_routes * capacity + ranks


def body(
    query_rows, key_rows, value_rows, query_gain, key_gain, moe_tokens, norm_gain, routes,
    route_weights, expert_gate, expert_up, expert_down, shared_gate, shared_up, shared_down,
):
    tok_rows, model_width = moe_tokens.shape
    lane = lax.axis_index("tp")
    values32 = moe_tokens.astype(F32)
    normed = (
        values32
        * lax.rsqrt(jnp.mean(values32 * values32, axis=-1, keepdims=True) + epsilon)
        * norm_gain
    ).astype(BF16)
    own_routes = lax.dynamic_slice_in_dim(routes, lane * tok_rows, tok_rows, 0)
    own_weights = lax.dynamic_slice_in_dim(route_weights, lane * tok_rows, tok_rows, 0)
    own_gates = own_weights / jnp.sum(own_weights, axis=-1, keepdims=True) * routed_scale
    slots = slot_numbers(own_routes, N_EP, CAP)
    slot_ids = jnp.arange(N_EP * CAP, dtype=jnp.int32)
    placing = jnp.any(slot_ids[:, None, None] == slots[None, :, :], axis=2).astype(BF16)
    send = jnp.dot(placing, normed, preferred_element_type=F32).astype(BF16)
    send = send.reshape(N_EP, CAP, model_width)
    choose = (slots.T[:, :, None] == slot_ids[None, None, :]).astype(BF16)
    q, kv = prepared(query_rows, key_rows, value_rows, query_gain, key_gain)
    attn_out, moe_out = layer(
        q, kv, send, normed, choose, own_gates,
        expert_gate[0], expert_up[0], expert_down[0], shared_gate, shared_up, shared_down,
    )
    return attn_out, moe_out


def solution(mesh):
    return jax.shard_map(
        body,
        mesh=mesh,
        in_specs=(
            P("ep", "tp"), P("ep", "tp"), P("ep", "tp"), P(), P(),
            P(("ep", "tp"), None), P(), P("ep", None), P("ep", None),
            P("ep", None, "tp"), P("ep", None, "tp"), P("ep", "tp", None),
            P(None, "tp"), P(None, "tp"), P("tp", None),
        ),
        out_specs=(P("ep", "tp"), P(("ep", "tp"), None)),
        check_vma=False,
    )
```

profile of v0, /device:TPU:96, one launch (start us, length us, event | category | flops | bytes accessed | tf_op | source)
XLA Modules:
  0.0 182.3 jit_solution(10434928031360066526)
XLA Ops:
  0.7 1.3 fusion.1
  2.0 0.7 constant_dynamic-slice_fusion.1
  2.7 0.7 tile.24
  3.3 0.6 tile.25.qg_ref
  3.9 0.7 tile.26
  4.6 0.6 tile.27.kg_ref
  5.2 0.7 fusion.13
  5.9 0.1 fusion.7
  6.1 0.7 convert_add_fusion
  6.9 0.1 fusion.8
  7.1 0.8 copy.34.sin_ref
  8.0 0.8 copy.33.cos_ref
  8.8 0.1 copy.36
  8.9 0.7 divide_multiply_fusion.gates_ref
  9.6 0.1 copy.31
  9.7 0.1 copy.32
  9.8 0.7 pad_maximum_fusion.kv_ref
  10.6 2.5 %prep.1 = (bf16[1024,128]{1,0:T(8,128)(2,1)}, bf16[256,128]{1,0:T(8,128)(2,1)}) custom-call(bf16[256,256]{1,0:T(8,128)(2,1)} %q_ref.1, bf16[256,128]{1,0:T(8,128)(2,1)} %pad_maximum_fusion.kv_ref, f32[1,128]{1,0:T(1,128)} %tile.25.qg_ref, f32[1,128]{1,0:T(1,128)} %tile.27.kg_ref, f32[256,128]{1,0:T(8,128)} %copy.33.cos_ref, f32[256,128]{1,0:T(8,128)} %copy.34.sin_ref), custom_call_target="tpu_custom_call" | custom-call | tf_op jit(solution)/shard_map/prep/pallas_call | solution.py:65
  13.1 0.8 fusion.5.choose_ref
  13.9 0.2 fusion.3.normed_ref
  14.1 2.1 %fusion.send_ref = bf16[64,8,2048]{2,1,0:T(8,128)(2,1)} fusion(pred[512,128]{1,0:T(8,128)(4,1)S(1)} %fusion.4, bf16[128,2048]{1,0:T(8,128)(2,1)S(1)} %fusion.3.normed_ref), kind=kOutput, calls=%fused_computation.1 | convolution fusion | flops 269484032 | bytes 2686976 | tf_op jit(solution)/shard_map/dot_general | solution.py:472
  16.2 162.7 %layer.1 = (bf16[256,256]{1,0:T(8,128)(2,1)}, bf16[128,2048]{1,0:T(8,128)(2,1)}) custom-call(bf16[1024,128]{1,0:T(8,128)(2,1)} %get-tuple-element.4.q_ref, bf16[256,128]{1,0:T(8,128)(2,1)} %get-tuple-element.5.kv_ref, bf16[64,8,2048]{2,1,0:T(8,128)(2,1)} %fusion.send_ref, bf16[128,2048]{1,0:T(8,128)(2,1)} %copy-done, bf16[2,128,512]{2,1,0:T(8,128)(2,1)} %fusion.5.choose_ref, ...), custom_call_target="tpu_custom_call" | custom-call | tf_op jit(solution)/shard_map/layer/pallas_call | solution.py:405
  178.9 1.6 copy.40
  180.4 1.9 %copy.41 = bf16[128,2048]{1,0:T(8,128)(2,1)} copy(bf16[128,2048]{1,0:T(8,128)(2,1)} %get-tuple-element.17) | data formatting | bytes 1048576
  (23 shorter events, 0.4 us)
Async XLA Ops:
  0.6 13.3 %copy-start.1 = (bf16[128,2048]{1,0:T(8,128)(2,1)S(1)}, bf16[128,2048]{1,0:T(8,128)(2,1)}, u32[]{:S(2)}) copy-start(bf16[128,2048]{1,0:T(8,128)(2,1)} %param.20) | copy-start | bytes 1572868
  0.6 13.3 %copy-start.4 = (f32[2048]{0:T(1024)S(1)}, f32[2048]{0:T(1024)}, u32[]{:S(2)}) copy-start(f32[2048]{0:T(1024)} %param.21) | copy-start | bytes 24580
  0.7 9.1 %copy-start.3 = (bf16[256,64]{0,1:T(8,128)(2,1)S(1)}, bf16[256,64]{0,1:T(8,128)(2,1)}, u32[]{:S(2)}) copy-start(bf16[256,64]{0,1:T(8,128)(2,1)} %param.17) | copy-start | bytes 98308
  0.7 8.9 %copy-start.2 = (bf16[256,64]{0,1:T(8,128)(2,1)S(1)}, bf16[256,64]{0,1:T(8,128)(2,1)}, u32[]{:S(2)}) copy-start(bf16[256,64]{0,1:T(8,128)(2,1)} %param.16) | copy-start | bytes 98308
  14.1 2.1 %copy-start = (bf16[128,2048]{1,0:T(8,128)(2,1)}, bf16[128,2048]{1,0:T(8,128)(2,1)S(1)}, u32[]{:S(2)}) copy-start(bf16[128,2048]{1,0:T(8,128)(2,1)S(1)} %fusion.3.normed_ref) | copy-start | bytes 1572868
where the time goes:
time: 183 us; the launch traced here: 182 us
  Pallas kernels  165 us (90%)
  local copies, waits for them, and re-layouts  8.69 us (5%)
  other arithmetic  5.46 us (3%)
  matrix products  2.19 us (1%)
    pallas_call x1, Pallas kernels, layer(): pl.pallas_call(layer_kernel, out_shape=[jax.ShapeDtypeStruct((256, 256),...  163 us
    unnamed x15, local copies, waits for them, and re-layouts  3.81 us

commit v1 on v0

--- a/solution.py
+++ b/solution.py
@@ -2,12 +2,14 @@
 
 import jax
 import jax.numpy as jnp
+import numpy as np
 from jax import lax
 from jax.experimental import pallas as pl
 from jax.experimental.pallas import tpu as pltpu
 from jax.sharding import PartitionSpec as P
 
 GRID_W = 64
+TOKENS_A = 16384
 MESH = pl.DeviceIdType.MESH
 F32 = jnp.float32
 BF16 = jnp.bfloat16
@@ -23,60 +25,17 @@
 NT = (((1,), (1,)), ((), ()))
 
 
-def prep_kernel(q_ref, kv_ref, qg_ref, kg_ref, cos_ref, sin_ref, qo_ref, kvo_ref):
-    rows = q_ref.shape[0]
-    lane = lax.broadcasted_iota(jnp.int32, (rows, 128), 1)
-    low = lane < 64
-    even = lax.rem(lane, 2) == 0
-    cosine, sine = cos_ref[...], sin_ref[...]
-
-    def turned(x, gain):
-        squares = x * x
-        first = jnp.sum(jnp.where(low, squares, 0.0), axis=1, keepdims=True) / 64.0
-        second = jnp.sum(jnp.where(low, 0.0, squares), axis=1, keepdims=True) / 64.0
-        inverse = jnp.where(low, lax.rsqrt(first + epsilon), lax.rsqrt(second + epsilon))
-        y = x * inverse * gain
-        partner = jnp.where(even, -pltpu.roll(y, 127, 1), pltpu.roll(y, 1, 1))
-        return (y * cosine + partner * sine).astype(BF16).astype(F32)
-
-    gain = qg_ref[...]
-    for pair in range(q_ref.shape[1] // 128):
-        x = q_ref[:, pair * 128 : pair * 128 + 128].astype(F32)
-        out = turned(x, gain) * 0.125
-        base = 2 * pair * rows
-        qo_ref[base : base + rows, :] = jnp.where(low, out, 0.0).astype(BF16)
-        qo_ref[base + rows : base + 2 * rows, :] = jnp.where(
-            low, pltpu.roll(out, 64, 1), 0.0
-        ).astype(BF16)
-    kv = kv_ref[...].astype(F32)
-    kvo_ref[...] = jnp.where(low, turned(kv, kg_ref[...]), kv).astype(BF16)
-
-
-def prepared(query_rows, key_rows, value_rows, query_gain, key_gain):
-    rows = query_rows.shape[0]
-    positions = lax.axis_index("ep") * rows + jnp.arange(rows, dtype=jnp.int32)
-    pair_count = 16
-    inv_freq = rotary_base ** (-jnp.arange(pair_count, dtype=F32) / pair_count)
-    grid_row = (positions // GRID_W).astype(F32)
-    grid_col = (positions % GRID_W).astype(F32)
-    angles = jnp.concatenate([grid_row[:, None] * inv_freq, grid_col[:, None] * inv_freq], axis=-1)
-    angles = jnp.tile(jnp.repeat(angles, 2, axis=1), (1, 2))
-    kv = jnp.concatenate([key_rows, value_rows], axis=1)
-    return pl.pallas_call(
-        prep_kernel,
-        out_shape=[
-            jax.ShapeDtypeStruct((4 * rows, 128), BF16),
-            jax.ShapeDtypeStruct((rows, 128), BF16),
-        ],
-        name="prep",
-    )(
-        query_rows,
-        kv,
-        jnp.tile(query_gain[None, :], (1, 2)),
-        jnp.tile(key_gain[None, :], (1, 2)),
-        jnp.cos(angles),
-        jnp.sin(angles),
-    )
+def angle_tables():
+    pairs = np.arange(128) % 64 // 2
+    inv_freq = (rotary_base ** (-np.arange(16, dtype=np.float64) / 16)).astype(np.float32)
+    freq = inv_freq[pairs % 16]
+    sign = np.where(np.arange(128) % 2 == 0, -1.0, 1.0)
+    tables = []
+    for count, mask in ((TOKENS_A // GRID_W, pairs < 16), (GRID_W, pairs >= 16)):
+        angles = (np.arange(count, dtype=np.float32)[:, None] * freq).astype(np.float64)
+        tables.append((np.cos(angles) * mask).astype(np.float32))
+        tables.append((np.sin(angles) * sign * mask).astype(np.float32))
+    return tables
 
 
 def silu_times(gate, up):
@@ -84,9 +43,11 @@
 
 
 def layer_kernel(
-    q_ref, kv_ref, send_ref, normed_ref, choose_ref, gates_ref,
+    query_ref, key_ref, value_ref, qgain_ref, kgain_ref, rcos_ref, rsin_ref, ccos_ref, csin_ref,
+    tokens_ref, ngain_ref, routes_ref, scores_ref,
     wg_ref, wu_ref, wd_ref, sg_ref, su_ref, sd_ref,
     attn_ref, moe_ref,
+    q_ref, normed_ref, send_ref, choose_ref, gates_ref,
     kvb, run_max, run_sum, mixed,
     wgb, wub, wdb, nall, arrived, rows_bf, hidden, outbuf, ret,
     sgb, sub, sdb, part, parts,
@@ -157,7 +118,7 @@
         item_copy(i, 2).start()
         item_copy(i, 1).wait_recv()
         item_copy(i, 3).start()
-        begin(i + 2)
+        begin(i + 3)
 
     def complete(i):
         item_copy(i, 2).wait_recv()
@@ -165,29 +126,98 @@
 
     begin(0)
     begin(1)
-
-    local = [pltpu.make_async_copy(kv_ref, kvb.at[c, x, z], own_sem.at[0])]
+    begin(2)
+
+    rows = query_ref.shape[0]
+    lanes = lax.broadcasted_iota(jnp.int32, (rows, 128), 1)
+    low, even = lanes < 64, lax.rem(lanes, 2) == 0
+    grid_rows = rows // GRID_W
+
+    def table(row_ref, col_ref):
+        return jnp.concatenate(
+            [row_ref[pl.ds(me * grid_rows + n, 1), :] + col_ref[...] for n in range(grid_rows)], axis=0
+        )
+
+    cosine, sine = table(rcos_ref, ccos_ref), table(rsin_ref, csin_ref)
+
+    def turned(values, gain):
+        squares = values * values
+        first = jnp.sum(jnp.where(low, squares, 0.0), axis=1, keepdims=True) / 64.0
+        second = jnp.sum(jnp.where(low, 0.0, squares), axis=1, keepdims=True) / 64.0
+        inverse = jnp.where(low, lax.rsqrt(first + epsilon), lax.rsqrt(second + epsilon))
+        y = values * inverse * gain
+        partner = jnp.where(even, pltpu.roll(y, 127, 1), pltpu.roll(y, 1, 1))
+        return (y * cosine + partner * sine).astype(BF16).astype(F32)
+
+    def both(gain_ref):
+        return jnp.concatenate([gain_ref[...], gain_ref[...]], axis=1)
+
+    kv = jnp.concatenate([key_ref[...].astype(F32), value_ref[...].astype(F32)], axis=0).T
+    kvb[c, x, z] = jnp.where(low, turned(kv, both(kgain_ref)), kv).astype(BF16)
+
+    def along_z(i):
+        return remote(
+            kvb.at[c, x, z], kvb.at[c, x, z], kv_send.at[i], kv_recv.at[i],
+            "ep", at(lax.rem(z + i, N_Z), x, c),
+        )
+
+    for i in range(1, N_Z):
+        along_z(i).start()
+
+    local = []
     for n, (src, dst) in enumerate((
         (wg_ref, wgb.at[0]), (wu_ref, wub.at[0]), (sg_ref, sgb), (su_ref, sub), (sd_ref, sdb),
-        (normed_ref, nall.at[0]), (send_ref.at[me], arrived.at[me]),
     )):
-        local.append(pltpu.make_async_copy(src, dst, own_sem.at[n + 1]))
+        local.append(pltpu.make_async_copy(src, dst, own_sem.at[n]))
     for j in range(CHUNKS):
         local.append(pltpu.make_async_copy(
             wd_ref.at[:, pl.ds(j * 512, 512)], wdb.at[0, j], own_sem.at[8 + j]
         ))
-
-    def along_z(i):
-        return remote(
-            kv_ref, kvb.at[c, x, z], kv_send.at[i], kv_recv.at[i],
-            "ep", at(lax.rem(z + i, N_Z), x, c),
-        )
-
-    local[0].start()
-    for i in range(1, N_Z):
-        along_z(i).start()
-    for copy in local[1:]:
+    for copy in local:
         copy.start()
+
+    gain = both(qgain_ref)
+    for pair in range(2):
+        values = query_ref[:, pair * 128 : pair * 128 + 128].astype(F32)
+        out = turned(values, gain) * 0.125
+        base = 2 * pair * rows
+        q_ref[base : base + rows, :] = jnp.where(low, out, 0.0).astype(BF16)
+        q_ref[base + rows : base + 2 * rows, :] = jnp.where(
+            low, pltpu.roll(out, 64, 1), 0.0
+        ).astype(BF16)
+
+    values = tokens_ref[...].astype(F32)
+    normed_ref[...] = (
+        values
+        * lax.rsqrt(jnp.mean(values * values, axis=-1, keepdims=True) + epsilon)
+        * ngain_ref[...]
+    ).astype(BF16)
+    own_rows = pl.ds(pl.multiple_of(lane * 128, 128), 128)
+    routes = routes_ref[:, own_rows]
+    expert_ids = lax.broadcasted_iota(jnp.int32, (N_EP, 128), 0)
+    named = [expert_ids == routes[k : k + 1, :] for k in range(2)]
+    counts = jnp.where(named[0] | named[1], 1.0, 0.0).astype(BF16)
+    square = (128, 128)
+    before = jnp.where(
+        lax.broadcasted_iota(jnp.int32, square, 0) < lax.broadcasted_iota(jnp.int32, square, 1), 1.0, 0.0
+    ).astype(BF16)
+    earlier = jnp.dot(counts, before, preferred_element_type=F32)
+    slot_ids = lax.broadcasted_iota(jnp.int32, (N_EP * CAP, 128), 0).astype(F32)
+    placing = 0.0
+    for k in range(2):
+        rank = jnp.sum(jnp.where(named[k], earlier, 0.0), axis=0, keepdims=True)
+        place = jnp.where(slot_ids == routes[k : k + 1, :].astype(F32) * CAP + rank, 1.0, 0.0)
+        placing = placing + place
+        choose_ref[k] = place.T.astype(BF16)
+    send_ref[...] = jnp.dot(
+        placing.astype(BF16), normed_ref[...], preferred_element_type=F32
+    ).reshape(N_EP, CAP, -1).astype(BF16)
+    scores = scores_ref[:, own_rows]
+    gates = scores / (scores[0:1] + scores[1:2]) * routed_scale
+    for k in range(2):
+        gates_ref[k] = jnp.broadcast_to(gates[k : k + 1], square).T
+    arrived[me] = send_ref[me]
+    nall[0] = normed_ref[...]
 
     x_next, x_prev = lax.rem(x + 1, N_X), lax.rem(x + 3, N_X)
     x_far = lax.rem(x + 2, N_X)
@@ -210,7 +240,6 @@
 
     blocks = (x, x_next, x_prev, x_far)
 
-    local[0].wait()
     for i in range(1, N_Z):
         along_z(i).wait_recv()
     to_next.start()
@@ -244,6 +273,7 @@
 
         @pl.when(t == 2)
         def _():
+            service(1)
             to_prev.wait_recv()
             on_prev.start()
             to_core(x_next, 1).start()
@@ -253,22 +283,25 @@
 
         @pl.when(t == 3)
         def _():
-            service(1)
             to_core(x_next, 1).wait_recv()
 
+        @pl.when(t == 4)
+        def _():
+            service(2)
+
         @pl.when(t == 5)
         def _():
             to_core(x_prev, 2).wait_recv()
 
         @pl.when(t == 6)
         def _():
+            service(3)
             on_next.wait_recv()
             on_prev.wait_recv()
             to_core(x_far, 3).start()
 
         @pl.when(t == 7)
         def _():
-            service(2)
             to_core(x_far, 3).wait_recv()
 
         keys = kvb[core, block].reshape(N_Z * 256, 128)
@@ -291,7 +324,6 @@
 
     lax.fori_loop(0, 8, attention_step, 0)
 
-    low = lax.broadcasted_iota(jnp.int32, (256, 128), 1) < 64
     for pair in range(2):
         base = pair * 512
         halves = []
@@ -302,8 +334,8 @@
             low, pltpu.roll(halves[0], 64, 1), halves[1]
         ).astype(BF16)
 
-    service(3)
-    for copy in local[1:]:
+    service(4)
+    for copy in local:
         copy.wait()
     remote(
         send_ref.at[pl.ds(0, N_EP - 1)], arrived.at[pl.ds(0, N_EP - 1)],
@@ -313,7 +345,7 @@
 
     for slot in range(N_TP):
         if slot == 2:
-            service(4)
+            service(5)
         if slot == 3:
             for i in range(4):
                 complete(i)
@@ -334,7 +366,8 @@
 
     back = []
     for j in range(CHUNKS):
-        service(5 + j)
+        if j < 3:
+            service(6 + j)
         complete(4 + j)
         total = jnp.zeros((N_EP * CAP, 512), F32)
         for slot in range(N_TP):
@@ -381,7 +414,7 @@
             total = total + parts[slot, :, columns].astype(F32)
         for k in range(2):
             picked = jnp.dot(choose_ref[k], flat, preferred_element_type=F32)
-            total = total + gates_ref[:, k : k + 1] * picked
+            total = total + gates_ref[k, :, 0:1] * picked
         moe_ref[:, columns] = total.astype(BF16)
 
     for i in range(len(items)):
@@ -397,20 +430,25 @@
         shares[slot].wait_send()
 
 
-def layer(q, kv, send, normed, choose, gates, wg, wu, wd, sg, su, sd):
+def layer(tokens, small, weights):
     vmem = pl.BlockSpec(memory_space=pltpu.VMEM)
     anywhere = pl.BlockSpec(memory_space=pl.ANY)
-    width = normed.shape[1]
+    width = tokens.shape[1]
     dma = pltpu.SemaphoreType.DMA
     return pl.pallas_call(
         layer_kernel,
         out_shape=[
             jax.ShapeDtypeStruct((256, 256), BF16),
-            jax.ShapeDtypeStruct(normed.shape, BF16),
+            jax.ShapeDtypeStruct(tokens.shape, BF16),
         ],
-        in_specs=[vmem, anywhere, anywhere, anywhere, vmem, vmem] + [anywhere] * 6,
+        in_specs=[vmem] * len(small) + [anywhere] * len(weights),
         out_specs=[vmem, vmem],
         scratch_shapes=[
+            pltpu.VMEM((1024, 128), BF16),
+            pltpu.VMEM((128, width), BF16),
+            pltpu.VMEM((N_EP, CAP, width), BF16),
+            pltpu.VMEM((2, 128, N_EP * CAP), BF16),
+            pltpu.VMEM((2, 128, 128), F32),
             pltpu.VMEM((N_CORE, N_X, N_Z, 256, 128), BF16),
             pltpu.VMEM((1024, 128), F32),
             pltpu.VMEM((1024, 128), F32),
@@ -437,47 +475,22 @@
             collective_id=1, has_side_effects=True, vmem_limit_bytes=60 * 1024 * 1024
         ),
         name="layer",
-    )(q, kv, send, normed, choose, gates, wg, wu, wd, sg, su, sd)
-
-
-def slot_numbers(own_routes, experts, capacity):
-    tok_rows = own_routes.shape[0]
-    named = own_routes[:, :, None] == jnp.arange(experts, dtype=jnp.int32)
-    counts = jnp.any(named, axis=1).astype(BF16)
-    rows = jnp.arange(tok_rows, dtype=jnp.int32)
-    before = (rows[:, None] > rows[None, :]).astype(BF16)
-    earlier = jnp.dot(before, counts, preferred_element_type=F32)
-    ranks = jnp.sum(jnp.where(named, earlier[:, None, :], 0.0), axis=2).astype(jnp.int32)
-    return own_routes * capacity + ranks
+    )(*small, *weights)
 
 
 def body(
     query_rows, key_rows, value_rows, query_gain, key_gain, moe_tokens, norm_gain, routes,
     route_weights, expert_gate, expert_up, expert_down, shared_gate, shared_up, shared_down,
 ):
-    tok_rows, model_width = moe_tokens.shape
-    lane = lax.axis_index("tp")
-    values32 = moe_tokens.astype(F32)
-    normed = (
-        values32
-        * lax.rsqrt(jnp.mean(values32 * values32, axis=-1, keepdims=True) + epsilon)
-        * norm_gain
-    ).astype(BF16)
-    own_routes = lax.dynamic_slice_in_dim(routes, lane * tok_rows, tok_rows, 0)
-    own_weights = lax.dynamic_slice_in_dim(route_weights, lane * tok_rows, tok_rows, 0)
-    own_gates = own_weights / jnp.sum(own_weights, axis=-1, keepdims=True) * routed_scale
-    slots = slot_numbers(own_routes, N_EP, CAP)
-    slot_ids = jnp.arange(N_EP * CAP, dtype=jnp.int32)
-    placing = jnp.any(slot_ids[:, None, None] == slots[None, :, :], axis=2).astype(BF16)
-    send = jnp.dot(placing, normed, preferred_element_type=F32).astype(BF16)
-    send = send.reshape(N_EP, CAP, model_width)
-    choose = (slots.T[:, :, None] == slot_ids[None, None, :]).astype(BF16)
-    q, kv = prepared(query_rows, key_rows, value_rows, query_gain, key_gain)
-    attn_out, moe_out = layer(
-        q, kv, send, normed, choose, own_gates,
+    small = (
+        query_rows, key_rows.T, value_rows.T, query_gain[None, :], key_gain[None, :],
+        *(jnp.asarray(table) for table in angle_tables()),
+        moe_tokens, norm_gain[None, :], routes.T, route_weights.T,
+    )
+    weights = (
         expert_gate[0], expert_up[0], expert_down[0], shared_gate, shared_up, shared_down,
     )
-    return attn_out, moe_out
+    return tuple(layer(moe_tokens, small, weights))
 
 
 def solution(mesh):

time: 183 us -> 164 us (0.90)
  the two profiles are of different devices: /device:TPU:96 before, /device:TPU:65 now
where the time goes in v1:
time: 164 us; the launch traced here: 161 us
  Pallas kernels  157 us (96%)
  local copies, waits for them, and re-layouts  3.45 us (2%)
    pallas_call x1, Pallas kernels, layer(): pl.pallas_call(layer_kernel, out_shape=[jax.ShapeDtypeStruct((256, 256),...  157 us
    unnamed x2, local copies, waits for them, and re-layouts  3.45 us

profile of v1, /device:TPU:65, one launch (start us, length us, event | category | flops | bytes accessed | tf_op | source)
XLA Modules:
  0.0 161.1 jit_solution(8223165314327059240)
XLA Ops:
  0.6 157.0 %layer.1 = (bf16[256,256]{1,0:T(8,128)(2,1)}, bf16[128,2048]{1,0:T(8,128)(2,1)}) custom-call(bf16[256,256]{1,0:T(8,128)(2,1)} %query_ref.1, bf16[64,256]{1,0:T(8,128)(2,1)} %bitcast.13, bf16[64,256]{1,0:T(8,128)(2,1)} %bitcast.14, f32[1,64]{1,0:T(1,128)} %bitcast.18, f32[1,64]{1,0:T(1,128)} %bitcast.19, f32[256,128]{1,0:T(8,128)} %constant.8.clone.rcos_ref, ...), custom_call_target="tpu_custom_call" | custom-call | tf_op jit(solution)/shard_map/layer/pallas_call | solution.py:438
  157.6 1.6 copy.23
  159.2 1.9 %copy.24 = bf16[128,2048]{1,0:T(8,128)(2,1)} copy(bf16[128,2048]{1,0:T(8,128)(2,1)} %get-tuple-element.5) | data formatting | bytes 1048576

commit v2 on v1

--- a/solution.py
+++ b/solution.py
@@ -21,7 +21,7 @@
 N_Z, N_X, N_CORE = 8, 4, 2
 N_EP, N_TP = 64, 4
 CAP = 8
-CHUNKS = 4
+CHUNKS = ((0, 256), (256, 256), (512, 512), (1024, 512), (1536, 512))
 NT = (((1,), (1,)), ((), ()))
 
 
@@ -46,13 +46,14 @@
     query_ref, key_ref, value_ref, qgain_ref, kgain_ref, rcos_ref, rsin_ref, ccos_ref, csin_ref,
     tokens_ref, ngain_ref, routes_ref, scores_ref,
     wg_ref, wu_ref, wd_ref, sg_ref, su_ref, sd_ref,
-    attn_ref, moe_ref,
-    q_ref, normed_ref, send_ref, choose_ref, gates_ref,
+    attn_out, moe_out,
+    attn_ref, moe_ref, q_ref, normed_ref, send_ref, choose_ref, gates_ref,
     kvb, run_max, run_sum, mixed,
-    wgb, wub, wdb, nall, arrived, rows_bf, hidden, outbuf, ret,
-    sgb, sub, sdb, part, parts,
+    wgb, wub, wdb, arrived, rows_bf, hidden, outbuf, ret,
+    sgb, sub, sdb, shared,
     item_send, item_recv, kv_send, kv_recv, x_send, x_recv, core_send, core_recv,
-    disp_send, disp_recv, ret_send, ret_recv, rs_send, rs_recv, own_sem,
+    disp_send, disp_recv, ret_send, ret_recv, unit_send, unit_recv, ring_send, ring_recv,
+    wide_send, wide_recv, pair_send, pair_recv, own_sem,
 ):
     me, lane = lax.axis_index("ep"), lax.axis_index("tp")
     z, x, c = lax.div(me, 8), lax.rem(lax.div(me, 2), 4), lax.rem(me, 2)
@@ -87,18 +88,16 @@
     for ref, buf in ((wg_ref, wgb), (wu_ref, wub)):
         for h in range(2):
             items.append((ref.at[pl.ds(h * 1024, 1024)], buf, (pl.ds(h * 1024, 1024),), h * 1024, 512))
-    for j in range(CHUNKS):
-        items.append((wd_ref.at[:, pl.ds(j * 512, 512)], wdb, (j,), 0, 128))
-    items.append((normed_ref, nall, (), 0, 64))
+    for first, count in CHUNKS:
+        items.append((wd_ref.at[:, pl.ds(first, count)], wdb, (slice(None), pl.ds(first, count)), 0, 128))
 
     def item_copy(i, n):
         src, buf, where, base, half = items[i]
-        lead = where[:-1] if where and not isinstance(where[0], int) else where
         s, r = item_send.at[i], item_recv.at[i]
         lower, upper = pl.ds(base, half), pl.ds(base + half, half)
 
         def piece(slot, rows):
-            return buf.at[(slot,) + lead + (rows,)]
+            return buf.at[(slot, rows) + where[1:]]
 
         if n == 0:
             return remote(src, buf.at[(1,) + where], s.at[0], r.at[0], "tp", right)
@@ -109,21 +108,58 @@
         return remote(piece(2, upper), piece(3, upper), s.at[3], r.at[3], "tp", left)
 
     def begin(i):
-        if i < len(items):
-            item_copy(i, 0).start()
-            item_copy(i, 1).start()
+        item_copy(i, 0).start()
+        item_copy(i, 1).start()
 
     def service(i):
         item_copy(i, 0).wait_recv()
         item_copy(i, 2).start()
         item_copy(i, 1).wait_recv()
         item_copy(i, 3).start()
-        begin(i + 3)
+        for later in follows.get(i, ()):
+            begin(later)
+
+    follows = {0: (3,), 3: (4, 5), 4: (6,), 5: (7,), 6: (8,)}
 
     def complete(i):
         item_copy(i, 2).wait_recv()
         item_copy(i, 3).wait_recv()
 
+    column = pl.ds(pl.multiple_of(((c * N_X + x) * 2 + lax.div(z, 4)) * 128, 128), 128)
+    bufs = (sgb, sub, sdb)
+    shares = (sg_ref.at[c, x, z], su_ref.at[c, x, z], sd_ref.at[lax.rem(z, 4), :, column])
+    others = pl.ds(1, N_TP - 1)
+
+    def unit_copy(b, slot):
+        peer = {1: right, 2: left, 3: opposite}[slot]
+        return remote(
+            shares[b], bufs[b].at[slot, c, x, z], unit_send.at[b, slot], unit_recv.at[b, slot], "tp", peer
+        )
+
+    def ring_copy(b, step, up):
+        origin = lax.rem(z + (N_Z - step + 1 if up else step - 1), N_Z)
+        ref = bufs[b].at[others, c, x, origin]
+        n = step - 1 if up else step + 3
+        to = lax.rem(z + (1 if up else N_Z - 1), N_Z)
+        return remote(ref, ref, ring_send.at[b, n], ring_recv.at[b, n], "ep", at(to, x, c))
+
+    ring_steps = ((1, True), (1, False), (2, True), (2, False), (3, True), (3, False), (4, True))
+
+    def ring_begin(step):
+        for b in range(3):
+            ring_copy(b, step, True).start()
+            if step < 4:
+                ring_copy(b, step, False).start()
+
+    def ring_finish(step):
+        for b in range(3):
+            ring_copy(b, step, True).wait_recv()
+            if step < 4:
+                ring_copy(b, step, False).wait_recv()
+
+    for slot in range(1, N_TP):
+        for b in range(3):
+            unit_copy(b, slot).start()
     begin(0)
     begin(1)
     begin(2)
@@ -166,15 +202,21 @@
 
     local = []
     for n, (src, dst) in enumerate((
-        (wg_ref, wgb.at[0]), (wu_ref, wub.at[0]), (sg_ref, sgb), (su_ref, sub), (sd_ref, sdb),
+        (wg_ref, wgb.at[0]), (wu_ref, wub.at[0]), (sg_ref, sgb.at[0]), (su_ref, sub.at[0]),
     )):
         local.append(pltpu.make_async_copy(src, dst, own_sem.at[n]))
-    for j in range(CHUNKS):
+    local.append(pltpu.make_async_copy(wd_ref, wdb.at[0], own_sem.at[4]))
+    for n in range(16):
         local.append(pltpu.make_async_copy(
-            wd_ref.at[:, pl.ds(j * 512, 512)], wdb.at[0, j], own_sem.at[8 + j]
+            sd_ref.at[:, :, pl.ds(n * 128, 128)],
+            sdb.at[0, n // 8, n // 2 % 4, pl.ds(n % 2 * 4, 4)], own_sem.at[16 + n],
         ))
     for copy in local:
         copy.start()
+    for slot in range(1, N_TP):
+        for b in range(3):
+            unit_copy(b, slot).wait_recv()
+    ring_begin(1)
 
     gain = both(qgain_ref)
     for pair in range(2):
@@ -217,7 +259,8 @@
     for k in range(2):
         gates_ref[k] = jnp.broadcast_to(gates[k : k + 1], square).T
     arrived[me] = send_ref[me]
-    nall[0] = normed_ref[...]
+    ring_finish(1)
+    ring_begin(2)
 
     x_next, x_prev = lax.rem(x + 1, N_X), lax.rem(x + 3, N_X)
     x_far = lax.rem(x + 2, N_X)
@@ -246,6 +289,25 @@
     to_prev.start()
     to_core(blocks[0], 0).start()
 
+    ring_finish(2)
+    ring_begin(3)
+
+    def wide_copy(b, n):
+        if n < 2:
+            ref = bufs[b].at[others, c, x]
+        elif n == 2:
+            ref = bufs[b].at[others, c, x_prev, low_z]
+        else:
+            ref = bufs[b].at[others, c, x_next, high_z]
+        return remote(ref, ref, wide_send.at[b, n], wide_recv.at[b, n], "ep", (up_x, down_x)[n % 2])
+
+    def pair_copy(b, n):
+        ref = bufs[b].at[others, c, blocks[n]]
+        return remote(ref, ref, pair_send.at[b, n], pair_recv.at[b, n], "ep", at(z, x, 1 - c))
+
+    ring_finish(3)
+    ring_begin(4)
+
     def dispatch(i, carry):
         peer = lax.rem(me + i, N_EP)
         remote(
@@ -284,6 +346,11 @@
         @pl.when(t == 3)
         def _():
             to_core(x_next, 1).wait_recv()
+            ring_finish(4)
+            for b in range(3):
+                wide_copy(b, 0).start()
+                wide_copy(b, 1).start()
+                pair_copy(b, 0).start()
 
         @pl.when(t == 4)
         def _():
@@ -333,8 +400,9 @@
         attn_ref[:, pair * 128 : pair * 128 + 128] = jnp.where(
             low, pltpu.roll(halves[0], 64, 1), halves[1]
         ).astype(BF16)
-
-    service(4)
+    leaving = [pltpu.make_async_copy(attn_ref, attn_out, own_sem.at[5])]
+    leaving[0].start()
+
     for copy in local:
         copy.wait()
     remote(
@@ -344,8 +412,6 @@
     rows_bf[...] = arrived[...].astype(F32).reshape(N_EP * CAP, -1).astype(BF16)
 
     for slot in range(N_TP):
-        if slot == 2:
-            service(5)
         if slot == 3:
             for i in range(4):
                 complete(i)
@@ -354,68 +420,68 @@
         up = jnp.dot(rows_in, wub[slot], preferred_element_type=F32)
         hidden[slot] = silu_times(gate, up)
 
+    columns = [pl.ds(first, count) for first, count in CHUNKS]
+
     def send_back(j):
         def one(i, carry):
             peer = lax.rem(me + i, N_EP)
             remote(
-                outbuf.at[j, peer], ret.at[j, me], ret_send.at[j], ret_recv.at[j], "ep", peer
+                outbuf.at[peer, :, columns[j]], ret.at[me, :, columns[j]],
+                ret_send.at[j], ret_recv.at[j], "ep", peer,
             ).start()
             return carry
 
         lax.fori_loop(1, N_EP, one, 0)
 
     back = []
-    for j in range(CHUNKS):
-        if j < 3:
-            service(6 + j)
+    for j, (first, count) in enumerate(CHUNKS):
+        service(4 + j)
         complete(4 + j)
-        total = jnp.zeros((N_EP * CAP, 512), F32)
+        total = jnp.zeros((N_EP * CAP, count), F32)
         for slot in range(N_TP):
             total = total + jnp.dot(
-                hidden[slot], wdb[slot, j], preferred_element_type=F32
+                hidden[slot], wdb[slot, :, first : first + count], preferred_element_type=F32
             ).astype(BF16).astype(F32)
-        outbuf[j] = total.reshape(N_EP, CAP, 512).astype(BF16)
+        outbuf[:, :, first : first + count] = total.reshape(N_EP, CAP, count).astype(BF16)
         send_back(j)
-        copy = pltpu.make_async_copy(outbuf.at[j, me], ret.at[j, me], own_sem.at[12 + j])
+        copy = pltpu.make_async_copy(
+            outbuf.at[me, :, columns[j]], ret.at[me, :, columns[j]], own_sem.at[8 + j]
+        )
         copy.start()
         back.append(copy)
-
-    def shared_of(slot):
-        rows_in = nall[slot]
-        gate = jnp.dot(rows_in, sgb[...], preferred_element_type=F32)
-        up = jnp.dot(rows_in, sub[...], preferred_element_type=F32)
-        return jnp.dot(silu_times(gate, up), sdb[...], preferred_element_type=F32).astype(BF16)
-
-    shares = {
-        1: remote(part.at[1], parts.at[2], rs_send.at[1], rs_recv.at[2], "tp", left),
-        2: remote(part.at[2], parts.at[1], rs_send.at[2], rs_recv.at[1], "tp", right),
-        3: remote(part.at[3], parts.at[3], rs_send.at[3], rs_recv.at[3], "tp", opposite),
-    }
-    for slot in (1, 2):
-        part[slot] = shared_of(slot)
-        shares[slot].start()
-    complete(8)
-    part[3] = shared_of(3)
-    shares[3].start()
-    part[0] = shared_of(0)
-    for slot in (1, 2, 3):
-        shares[slot].wait_recv()
-
-    for j in range(CHUNKS):
-        columns = slice(j * 512, j * 512 + 512)
-        back[j].wait()
-        remote(
-            outbuf.at[j, pl.ds(0, N_EP - 1)], ret.at[j, pl.ds(0, N_EP - 1)],
-            ret_send.at[j], ret_recv.at[j], "ep", up_x,
-        ).wait()
-        flat = ret[j].astype(F32).reshape(N_EP * CAP, 512).astype(BF16)
-        total = part[0, :, columns].astype(F32)
-        for slot in (1, 2, 3):
-            total = total + parts[slot, :, columns].astype(F32)
-        for k in range(2):
-            picked = jnp.dot(choose_ref[k], flat, preferred_element_type=F32)
-            total = total + gates_ref[k, :, 0:1] * picked
-        moe_ref[:, columns] = total.astype(BF16)
+        if j == 0:
+            for b in range(3):
+                wide_copy(b, 0).wait_recv()
+                wide_copy(b, 2).start()
+                pair_copy(b, 2).start()
+                wide_copy(b, 1).wait_recv()
+                wide_copy(b, 3).start()
+                pair_copy(b, 1).start()
+
+    for b in range(3):
+        wide_copy(b, 2).wait_recv()
+        wide_copy(b, 3).wait_recv()
+        pair_copy(b, 3).start()
+    for n in range(4):
+        for b in range(3):
+            pair_copy(b, n).wait_recv()
+    shared[...] = jnp.zeros_like(shared)
+
+    def shared_step(slot, carry):
+        rows_in = normed_ref[...]
+        gate = jnp.dot(rows_in, sgb[slot].reshape(-1, 256), preferred_element_type=F32)
+        up = jnp.dot(rows_in, sub[slot].reshape(-1, 256), preferred_element_type=F32)
+        units = silu_times(gate, up)
+        for n in range(16):
+            here = slice(n * 128, n * 128 + 128)
+            half = n % 2 * 4
+            down = sdb[slot, n // 8, n // 2 % 4, half : half + 4].reshape(256, 128)
+            shared[:, here] += jnp.dot(
+                units, down, preferred_element_type=F32
+            ).astype(BF16).astype(F32)
+        return carry
+
+    lax.fori_loop(0, N_TP, shared_step, 0)
 
     for i in range(len(items)):
         for n in range(4):
@@ -426,8 +492,34 @@
         copy.wait_send()
     for n in range(4):
         to_core(blocks[n], n).wait_send()
-    for slot in (1, 2, 3):
-        shares[slot].wait_send()
+    for b in range(3):
+        for slot in range(1, N_TP):
+            unit_copy(b, slot).wait_send()
+        for step, up in ring_steps:
+            ring_copy(b, step, up).wait_send()
+        for n in range(4):
+            wide_copy(b, n).wait_send()
+            pair_copy(b, n).wait_send()
+
+    for j, (first, count) in enumerate(CHUNKS):
+        here = slice(first, first + count)
+        back[j].wait()
+        remote(
+            outbuf.at[pl.ds(0, N_EP - 1), :, columns[j]], ret.at[pl.ds(0, N_EP - 1), :, columns[j]],
+            ret_send.at[j], ret_recv.at[j], "ep", up_x,
+        ).wait()
+        flat = ret[:, :, here].astype(F32).reshape(N_EP * CAP, count).astype(BF16)
+        total = shared[:, here]
+        for k in range(2):
+            picked = jnp.dot(choose_ref[k], flat, preferred_element_type=F32)
+            total = total + gates_ref[k, :, 0:1] * picked
+        moe_ref[:, here] = total.astype(BF16)
+        leaving.append(pltpu.make_async_copy(
+            moe_ref.at[:, columns[j]], moe_out.at[:, columns[j]], own_sem.at[32 + j]
+        ))
+        leaving[-1].start()
+    for copy in leaving:
+        copy.wait()
 
 
 def layer(tokens, small, weights):
@@ -442,8 +534,10 @@
             jax.ShapeDtypeStruct(tokens.shape, BF16),
         ],
         in_specs=[vmem] * len(small) + [anywhere] * len(weights),
-        out_specs=[vmem, vmem],
+        out_specs=[anywhere, anywhere],
         scratch_shapes=[
+            pltpu.VMEM((256, 256), BF16),
+            pltpu.VMEM((128, width), BF16),
             pltpu.VMEM((1024, 128), BF16),
             pltpu.VMEM((128, width), BF16),
             pltpu.VMEM((N_EP, CAP, width), BF16),
@@ -455,21 +549,20 @@
             pltpu.VMEM((1024, 128), F32),
             pltpu.VMEM((N_TP, width, 256), BF16),
             pltpu.VMEM((N_TP, width, 256), BF16),
-            pltpu.VMEM((N_TP, CHUNKS, 256, 512), BF16),
-            pltpu.VMEM((N_TP, 128, width), BF16),
+            pltpu.VMEM((N_TP, 256, width), BF16),
             pltpu.VMEM((N_EP, CAP, width), BF16),
             pltpu.VMEM((N_EP * CAP, width), BF16),
             pltpu.VMEM((N_TP, N_EP * CAP, 256), BF16),
-            pltpu.VMEM((CHUNKS, N_EP, CAP, 512), BF16),
-            pltpu.VMEM((CHUNKS, N_EP, CAP, 512), BF16),
-            pltpu.VMEM((width, 256), BF16),
-            pltpu.VMEM((width, 256), BF16),
-            pltpu.VMEM((256, width), BF16),
-            pltpu.VMEM((N_TP, 128, width), BF16),
-            pltpu.VMEM((N_TP, 128, width), BF16),
+            pltpu.VMEM((N_EP, CAP, width), BF16),
+            pltpu.VMEM((N_EP, CAP, width), BF16),
+            pltpu.VMEM((N_TP, N_CORE, N_X, N_Z, 32, 256), BF16),
+            pltpu.VMEM((N_TP, N_CORE, N_X, N_Z, 32, 256), BF16),
+            pltpu.VMEM((N_TP, N_CORE, N_X, N_Z, 64, 128), BF16),
+            pltpu.VMEM((128, width), F32),
             dma((9, 4)), dma((9, 4)), dma((N_Z,)), dma((N_Z,)), dma((4,)), dma((4,)),
-            dma((4,)), dma((4,)), dma((1,)), dma((1,)), dma((CHUNKS,)), dma((CHUNKS,)),
-            dma((4,)), dma((4,)), dma((16,)),
+            dma((4,)), dma((4,)), dma((1,)), dma((1,)), dma((len(CHUNKS),)), dma((len(CHUNKS),)),
+            dma((3, 4)), dma((3, 4)), dma((3, 8)), dma((3, 8)), dma((3, 4)), dma((3, 4)),
+            dma((3, 4)), dma((3, 4)), dma((40,)),
         ],
         compiler_params=pltpu.CompilerParams(
             collective_id=1, has_side_effects=True, vmem_limit_bytes=60 * 1024 * 1024
@@ -488,7 +581,9 @@
         moe_tokens, norm_gain[None, :], routes.T, route_weights.T,
     )
     weights = (
-        expert_gate[0], expert_up[0], expert_down[0], shared_gate, shared_up, shared_down,
+        expert_gate[0], expert_up[0], expert_down[0],
+        shared_gate.reshape(N_CORE, N_X, N_Z, 32, 256), shared_up.reshape(N_CORE, N_X, N_Z, 32, 256),
+        shared_down.reshape(4, 64, -1),
     )
     return tuple(layer(moe_tokens, small, weights))
 

time: 164 us -> 158 us (0.963); the launches traced: 161 us -> 158 us
  Pallas kernels: 157 us -> 154 us
    pallas_call x1, Pallas kernels: 157 us -> 154 us  [layer(): pl.pallas_call(layer_kernel, out_shape=[jax.ShapeDtypeStruct((256, 256),...]
where the time goes in v2:
time: 158 us
  Pallas kernels  154 us (97%)
  local copies, waits for them, and re-layouts  3.45 us (2%)
    pallas_call x1, Pallas kernels, layer(): pl.pallas_call(layer_kernel, out_shape=[jax.ShapeDtypeStruct((256, 256),...  154 us
    unnamed x2, local copies, waits for them, and re-layouts  3.45 us

profile of v2, /device:TPU:65, one launch (start us, length us, event | category | flops | bytes accessed | tf_op | source)
XLA Modules:
  0.0 157.9 jit_solution(7324370278763094936)
XLA Ops:
  0.6 153.8 %layer.1 = (bf16[256,256]{1,0:T(8,128)(2,1)}, bf16[128,2048]{1,0:T(8,128)(2,1)}) custom-call(bf16[256,256]{1,0:T(8,128)(2,1)} %query_ref.1, bf16[64,256]{1,0:T(8,128)(2,1)} %bitcast.19, bf16[64,256]{1,0:T(8,128)(2,1)} %bitcast.20, f32[1,64]{1,0:T(1,128)} %bitcast.24, f32[1,64]{1,0:T(1,128)} %bitcast.25, f32[256,128]{1,0:T(8,128)} %constant.8.clone.rcos_ref, ...), custom_call_target="tpu_custom_call" | custom-call | tf_op jit(solution)/shard_map/layer/pallas_call | solution.py:530
  154.5 1.6 copy.23
  156.0 1.9 %copy.24 = bf16[128,2048]{1,0:T(8,128)(2,1)} copy(bf16[128,2048]{1,0:T(8,128)(2,1)} %get-tuple-element.5) | data formatting | bytes 1048576

commit v3 on v2

--- a/solution.py
+++ b/solution.py
@@ -119,7 +119,7 @@
         for later in follows.get(i, ()):
             begin(later)
 
-    follows = {0: (3,), 3: (4, 5), 4: (6,), 5: (7,), 6: (8,)}
+    follows = {0: (3,), 3: (4,), 4: (5, 6), 5: (7,), 6: (8,)}
 
     def complete(i):
         item_copy(i, 2).wait_recv()
@@ -305,9 +305,6 @@
         ref = bufs[b].at[others, c, blocks[n]]
         return remote(ref, ref, pair_send.at[b, n], pair_recv.at[b, n], "ep", at(z, x, 1 - c))
 
-    ring_finish(3)
-    ring_begin(4)
-
     def dispatch(i, carry):
         peer = lax.rem(me + i, N_EP)
         remote(
@@ -315,7 +312,12 @@
         ).start()
         return carry
 
-    lax.fori_loop(1, N_EP, dispatch, 0)
+    lax.fori_loop(1, 9, dispatch, 0)
+
+    ring_finish(3)
+    ring_begin(4)
+
+    lax.fori_loop(9, N_EP, dispatch, 0)
 
     service(0)
 
@@ -413,6 +415,7 @@
 
     for slot in range(N_TP):
         if slot == 3:
+            service(4)
             for i in range(4):
                 complete(i)
         rows_in = rows_bf[...]
@@ -435,7 +438,8 @@
 
     back = []
     for j, (first, count) in enumerate(CHUNKS):
-        service(4 + j)
+        if j:
+            service(4 + j)
         complete(4 + j)
         total = jnp.zeros((N_EP * CAP, count), F32)
         for slot in range(N_TP):
@@ -449,14 +453,13 @@
         )
         copy.start()
         back.append(copy)
-        if j == 0:
-            for b in range(3):
-                wide_copy(b, 0).wait_recv()
-                wide_copy(b, 2).start()
-                pair_copy(b, 2).start()
-                wide_copy(b, 1).wait_recv()
-                wide_copy(b, 3).start()
-                pair_copy(b, 1).start()
+        for b in {1: (0, 1), 2: (2,)}.get(j, ()):
+            wide_copy(b, 0).wait_recv()
+            wide_copy(b, 2).start()
+            pair_copy(b, 2).start()
+            wide_copy(b, 1).wait_recv()
+            wide_copy(b, 3).start()
+            pair_copy(b, 1).start()
 
     for b in range(3):
         wide_copy(b, 2).wait_recv()

time: 158 us -> 159 us (level)
  no operation moved by 1% of the time
where the time goes in v3:
time: 159 us
  Pallas kernels  155 us (97%)
  local copies, waits for them, and re-layouts  3.45 us (2%)
    pallas_call x1, Pallas kernels, layer(): pl.pallas_call(layer_kernel, out_shape=[jax.ShapeDtypeStruct((256, 256),...  155 us
    unnamed x2, local copies, waits for them, and re-layouts  3.45 us

profile of v3, /device:TPU:65, one launch (start us, length us, event | category | flops | bytes accessed | tf_op | source)
XLA Modules:
  0.0 159.3 jit_solution(666034511034308764)
XLA Ops:
  0.6 155.2 %layer.1 = (bf16[256,256]{1,0:T(8,128)(2,1)}, bf16[128,2048]{1,0:T(8,128)(2,1)}) custom-call(bf16[256,256]{1,0:T(8,128)(2,1)} %query_ref.1, bf16[64,256]{1,0:T(8,128)(2,1)} %bitcast.19, bf16[64,256]{1,0:T(8,128)(2,1)} %bitcast.20, f32[1,64]{1,0:T(1,128)} %bitcast.24, f32[1,64]{1,0:T(1,128)} %bitcast.25, f32[256,128]{1,0:T(8,128)} %constant.8.clone.rcos_ref, ...), custom_call_target="tpu_custom_call" | custom-call | tf_op jit(solution)/shard_map/layer/pallas_call | solution.py:533
  155.9 1.6 copy.23
  157.4 1.9 %copy.24 = bf16[128,2048]{1,0:T(8,128)(2,1)} copy(bf16[128,2048]{1,0:T(8,128)(2,1)} %get-tuple-element.5) | data formatting | bytes 1048576

commit v4 on v3

--- a/solution.py
+++ b/solution.py
@@ -119,7 +119,7 @@
         for later in follows.get(i, ()):
             begin(later)
 
-    follows = {0: (3,), 3: (4,), 4: (5, 6), 5: (7,), 6: (8,)}
+    follows = {0: (3,), 3: (4, 5), 5: (6, 7), 6: (8,)}
 
     def complete(i):
         item_copy(i, 2).wait_recv()
@@ -416,6 +416,7 @@
     for slot in range(N_TP):
         if slot == 3:
             service(4)
+            service(5)
             for i in range(4):
                 complete(i)
         rows_in = rows_bf[...]
@@ -438,7 +439,7 @@
 
     back = []
     for j, (first, count) in enumerate(CHUNKS):
-        if j:
+        if j > 1:
             service(4 + j)
         complete(4 + j)
         total = jnp.zeros((N_EP * CAP, count), F32)

time: 159 us -> 156 us (0.981)
  Pallas kernels: 155 us -> 152 us
    pallas_call x1, Pallas kernels: 155 us -> 152 us  [layer(): pl.pallas_call(layer_kernel, out_shape=[jax.ShapeDtypeStruct((256, 256),...]
where the time goes in v4:
time: 156 us
  Pallas kernels  152 us (97%)
  local copies, waits for them, and re-layouts  3.45 us (2%)
    pallas_call x1, Pallas kernels, layer(): pl.pallas_call(layer_kernel, out_shape=[jax.ShapeDtypeStruct((256, 256),...  152 us
    unnamed x2, local copies, waits for them, and re-layouts  3.45 us

profile of v4, /device:TPU:65, one launch (start us, length us, event | category | flops | bytes accessed | tf_op | source)
XLA Modules:
  0.0 155.9 jit_solution(10503911067296218633)
XLA Ops:
  0.6 151.8 %layer.1 = (bf16[256,256]{1,0:T(8,128)(2,1)}, bf16[128,2048]{1,0:T(8,128)(2,1)}) custom-call(bf16[256,256]{1,0:T(8,128)(2,1)} %query_ref.1, bf16[64,256]{1,0:T(8,128)(2,1)} %bitcast.19, bf16[64,256]{1,0:T(8,128)(2,1)} %bitcast.20, f32[1,64]{1,0:T(1,128)} %bitcast.24, f32[1,64]{1,0:T(1,128)} %bitcast.25, f32[256,128]{1,0:T(8,128)} %constant.8.clone.rcos_ref, ...), custom_call_target="tpu_custom_call" | custom-call | tf_op jit(solution)/shard_map/layer/pallas_call | solution.py:534
  152.5 1.6 %copy.23 = bf16[256,256]{1,0:T(8,128)(2,1)} copy(bf16[256,256]{1,0:T(8,128)(2,1)} %get-tuple-element.4) | data formatting | bytes 262144
  154.0 1.9 %copy.24 = bf16[128,2048]{1,0:T(8,128)(2,1)} copy(bf16[128,2048]{1,0:T(8,128)(2,1)} %get-tuple-element.5) | data formatting | bytes 1048576
